TPU v7x, 512 devices: a whole 4x4x16 slice. The times are simulated.
512 devices in a mesh: ep: 128 (over z, x, core), tp: 4 (over y).
Axes of the slice: x: 4, y: 4, z: 16, core: 2. Of those that a mesh axis runs over, the one named last changes fastest.
Arguments:
- tokens: bfloat16 [1024, 1024], P('ep'), may hold values from -6 to 6
- lengths: int32 [1024], P('ep'), may hold values from 1 to 512, as said below
- cache_keys: bfloat16 [1024, 512, 4, 128], P('ep', None, 'tp'), may hold values from -2.5 to 2.5
- cache_values: bfloat16 [1024, 512, 4, 128], P('ep', None, 'tp'), may hold values from -6 to 6
- cache_cum: float32 [1024, 4, 512], P('ep', 'tp'), may hold values from -1536 to 0, as said below
- norm_gain: bfloat16 [1024], replicated, may hold values from 0.099609375 to 1.8984375
- query_weight: bfloat16 [1024, 1024], P(None, 'tp'), may hold values from -0.1875 to 0.1875
- key_weight: bfloat16 [1024, 512], P(None, 'tp'), may hold values from -0.1875 to 0.1875
- value_weight: bfloat16 [1024, 512], P(None, 'tp'), may hold values from -0.1875 to 0.1875
- forget_weight: bfloat16 [1024, 4], P(None, 'tp'), may hold values from -0.1875 to 0.1875
- forget_bias: float32 [4], P('tp'), may hold values from -1 to 2
- query_gain: bfloat16 [128], replicated, may hold values from 0.29882812 to 2.5
- key_gain: bfloat16 [128], replicated, may hold values from 0.099609375 to 1.8984375
- out_weight: bfloat16 [1024, 1024], P('tp'), may hold values from -0.1875 to 0.1875
- ffn_gain: bfloat16 [1024], replicated, may hold values from 0.099609375 to 1.8984375
- mix_weight: bfloat16 [1024], replicated, may hold values from -0.1875 to 0.1875
- shared_gate: bfloat16 [1024, 4096], P(None, 'ep'), may hold values from -0.1875 to 0.1875
- shared_up: bfloat16 [1024, 4096], P(None, 'ep'), may hold values from -0.1875 to 0.1875
- shared_down: bfloat16 [4096, 1024], P('ep', 'tp'), may hold values from -0.09375 to 0.09375
- routes: int32 [1024, 2], P('ep'), may hold values from 0 to 127, all different within a row; in each aligned block of 8 rows (0 to 7, 8 to 15, ...) at most 4 rows name the same one
- route_weights: float32 [1024, 2], P('ep'), may hold values from 0.1 to 1
- expert_gate: bfloat16 [128, 1024, 512], P('ep', None, 'tp'), may hold values from -0.1875 to 0.1875
- expert_up: bfloat16 [128, 1024, 512], P('ep', None, 'tp'), may hold values from -0.1875 to 0.1875
- expert_down: bfloat16 [128, 512, 1024], P('ep', 'tp'), may hold values from -0.25 to 0.25
Outputs:
- layer_out: bfloat16 [1024, 1024], P('ep', 'tp')
Inputs may be any that keep to these rules, and one draw needn't show every extreme that they name: `lengths`: at least one sequence has exactly 512 cached positions. `cache_cum`: along the positions each row never rises. `routes`: the 2 experts of a token differ; among the 8 rows of one device no expert is named by more than 4 rows, a bound that some block reaches.
All inputs are finite; a program needn't handle non-finite values.
Results may differ from a plain program's by a relative error of at most 0.013.
Values may be sent and summed in bfloat16 or wider, within the bound.
A program may use at most 64 MiB of HBM per device.

v0:
```python
import jax
import jax.numpy as jnp
from jax import lax
from jax.sharding import Mesh
from jax.sharding import PartitionSpec as P

CAP = 4
EP = ("ep_0", "ep_1", "ep_2")
epsilon = 1e-06


def copy_for_each(shard, axis):
    peers = lax.axis_size(axis)
    return lax.all_to_all(
        jnp.broadcast_to(shard[None], (peers, *shard.shape)), axis, 0, 0, tiled=True
    )


def of_everyone(shard, axis):
    return copy_for_each(shard, axis).astype(jnp.float32).sum(axis=0)


def cut_along(shard, dim, peers):
    before, after = (shard.shape[:dim], shard.shape[dim + 1 :])
    return jnp.moveaxis(shard.reshape(*before, peers, -1, *after), dim, 0)


def summed_on_arrival(shard, axis, dim):
    peers = lax.axis_size(axis)
    tiles = lax.all_to_all(cut_along(shard, dim, peers), axis, 0, 0, tiled=True)
    return jnp.sum(tiles.astype(jnp.float32), axis=0)


def sum_in_order(tiles, axes, sequence):
    shape = [lax.axis_size(a) for a in axes]
    tiles = tiles.reshape(*shape, *tiles.shape[1:])
    tiles = tiles.transpose(*sequence, *range(len(axes), tiles.ndim))
    tiles = tiles.reshape(-1, *tiles.shape[len(axes) :])
    for k in sequence:
        tiles = lax.psum_scatter(tiles, axes[k], scatter_dimension=0, tiled=True)
    return tiles[0]


def summed_rows(shard, axes, sequence, dim):
    peers = lax.axis_size(axes)
    return sum_in_order(cut_along(shard, dim, peers), axes, sequence)


def rms_norm(values, gain):
    values = values.astype(jnp.float32)
    return (
        values
        * lax.rsqrt(jnp.mean(values * values, axis=-1, keepdims=True) + epsilon)
        * gain.astype(jnp.float32)
    )


def per_device(
    tokens,
    lengths,
    cache_keys,
    cache_values,
    cache_cum,
    norm_gain,
    query_weight,
    key_weight,
    value_weight,
    forget_weight,
    forget_bias,
    query_gain,
    key_gain,
    out_weight,
    ffn_gain,
    mix_weight,
    shared_gate,
    shared_up,
    shared_down,
    routes,
    route_weights,
    expert_gate,
    expert_up,
    expert_down,
):
    seq_rows = tokens.shape[0]
    cache_len = cache_keys.shape[1]
    kv_local = cache_keys.shape[2]
    head_size = cache_keys.shape[3]
    normed = rms_norm(tokens, norm_gain).astype(jnp.bfloat16)
    query = jnp.dot(normed, query_weight, preferred_element_type=jnp.float32)
    query = rms_norm(query.reshape(seq_rows, kv_local, -1, head_size), query_gain).astype(
        jnp.bfloat16
    )
    new_key = jnp.dot(normed, key_weight, preferred_element_type=jnp.float32)
    new_key = rms_norm(new_key.reshape(seq_rows, kv_local, head_size), key_gain).astype(
        jnp.bfloat16
    )
    new_value = jnp.dot(normed, value_weight, preferred_element_type=jnp.float32).astype(
        jnp.bfloat16
    )
    new_value = new_value.reshape(seq_rows, kv_local, head_size)
    new_log = jax.nn.log_sigmoid(
        jnp.dot(normed, forget_weight, preferred_element_type=jnp.float32) + forget_bias
    )
    position = jnp.arange(cache_len, dtype=jnp.int32)
    live = position[None, :] < lengths[:, None]
    at_last = (position[None, :] == lengths[:, None] - 1)[:, None, :]
    last_cum = jnp.sum(jnp.where(at_last, cache_cum, 0.0), axis=-1)
    gate_bias = last_cum[:, :, None] - cache_cum + new_log[:, :, None]
    score_scale = head_size ** (-0.5)
    past = (
        jnp.einsum("skgd,spkd->skgp", query, cache_keys, preferred_element_type=jnp.float32)
        * score_scale
    )
    past = past + gate_bias[:, :, None, :]
    past = jnp.where(live[:, None, None, :], past, -jnp.inf)
    own = (
        jnp.sum(query.astype(jnp.float32) * new_key.astype(jnp.float32)[:, :, None, :], axis=-1)
        * score_scale
    )
    past_exp = jnp.exp(past)
    own_exp = jnp.exp(own)
    denominator = jnp.sum(past_exp, axis=-1) + own_exp
    past_prob = (past_exp / denominator[..., None]).astype(jnp.bfloat16)
    own_prob = (own_exp / denominator).astype(jnp.bfloat16)
    mixed = jnp.einsum(
        "skgp,spkd->skgd", past_prob, cache_values, preferred_element_type=jnp.float32
    )
    mixed = (
        mixed
        + own_prob.astype(jnp.float32)[..., None] * new_value.astype(jnp.float32)[:, :, None, :]
    )
    heads_out = mixed.astype(jnp.bfloat16).reshape(seq_rows, -1)
    partial_value = jnp.dot(heads_out, out_weight, preferred_element_type=jnp.float32)
    attended = of_everyone(partial_value.astype(jnp.bfloat16), "tp").astype(jnp.float32)
    residual = tokens.astype(jnp.float32) + attended
    ffn_in = rms_norm(residual, ffn_gain).astype(jnp.bfloat16)
    mix_gate = jax.nn.sigmoid(jnp.dot(ffn_in, mix_weight, preferred_element_type=jnp.float32))
    slice_width = ffn_in.shape[1] // lax.axis_size("tp")
    slice_start = lax.axis_index("tp") * slice_width
    ep_count = lax.axis_size(EP)
    local_experts = expert_gate.shape[0]
    num_experts = ep_count * local_experts
    topk = routes.shape[1]
    n_assign = seq_rows * topk
    order = jnp.arange(n_assign, dtype=jnp.int32)
    earlier = order[None, :] < order[:, None]
    slot_ids = jnp.arange(num_experts * CAP, dtype=jnp.int32)
    flat_route = routes.reshape(-1)
    same_expert = flat_route[:, None] == flat_route[None, :]
    slot_rank = jnp.sum(jnp.logical_and(same_expert, earlier), axis=1)
    slot_index = flat_route * CAP + slot_rank
    gathered_rows, gathered_routes = (
        lax.all_gather(ffn_in, EP, axis=0, tiled=True),
        lax.all_gather(routes, EP, axis=0, tiled=True),
    )
    pre_gate = jnp.dot(gathered_rows, shared_gate, preferred_element_type=jnp.float32)
    pre_up = jnp.dot(gathered_rows, shared_up, preferred_element_type=jnp.float32)
    shared_hidden = (jax.nn.silu(pre_gate) * pre_up).astype(jnp.bfloat16)
    terms = jnp.dot(shared_hidden, shared_down, preferred_element_type=jnp.float32)
    block_routes = gathered_routes.reshape(ep_count, n_assign)
    local_id = block_routes - lax.axis_index(EP) * local_experts
    mine = jnp.logical_and(local_id >= 0, local_id < local_experts)
    same_block = block_routes[:, :, None] == block_routes[:, None, :]
    block_rank = jnp.sum(jnp.logical_and(same_block, earlier[None, :, :]), axis=2)
    source = jnp.arange(ep_count, dtype=jnp.int32)[:, None]
    own_slot = source * (local_experts * CAP) + local_id * CAP + block_rank
    own_slot = jnp.where(mine, own_slot, -1).reshape(-1)
    pick_table = (own_slot[None, :] == slot_ids[:, None]).astype(jnp.bfloat16)
    repeated_all = jnp.repeat(gathered_rows, topk, axis=0)
    received = jnp.dot(pick_table, repeated_all, preferred_element_type=jnp.float32).astype(
        jnp.bfloat16
    )
    received = received.reshape(ep_count, local_experts, CAP, ffn_in.shape[1])
    pre_gate = jnp.einsum(
        "nekd,edf->nekf", received, expert_gate, preferred_element_type=jnp.float32
    )
    pre_up = jnp.einsum("nekd,edf->nekf", received, expert_up, preferred_element_type=jnp.float32)
    hidden = (jax.nn.silu(pre_gate) * pre_up).astype(jnp.bfloat16)
    part_out = jnp.einsum("nekf,efd->nekd", hidden, expert_down, preferred_element_type=jnp.float32)
    summed = summed_on_arrival(part_out.astype(jnp.bfloat16), "tp", 3)
    results = summed.astype(jnp.bfloat16)
    dense = summed_rows(terms, EP, (2, 0, 1), 0)
    returned = lax.all_to_all(results, EP, split_axis=0, concat_axis=0, tiled=True)
    returned = returned.reshape(num_experts * CAP, -1).astype(jnp.float32)
    norm_weights = route_weights / jnp.sum(route_weights, axis=1, keepdims=True)
    slot_table = slot_index.reshape(seq_rows, topk)
    combine = jnp.sum(
        (slot_table[:, :, None] == slot_ids[None, None, :]) * norm_weights[:, :, None], axis=1
    )
    routed = jnp.dot(combine, returned, precision=lax.Precision.HIGHEST)
    residual_slice = lax.dynamic_slice_in_dim(residual, slice_start, slice_width, 1)
    return (residual_slice + mix_gate[:, None] * dense + routed).astype(jnp.bfloat16)


def solution(mesh):
    finer = Mesh(mesh.devices.reshape(16, 4, 2, mesh.shape["tp"]), ("ep_0", "ep_1", "ep_2", "tp"))
    placed = (
        P(EP, None),
        P(EP),
        P(EP, None, "tp", None),
        P(EP, None, "tp", None),
        P(EP, "tp", None),
        P(),
        P(None, "tp"),
        P(None, "tp"),
        P(None, "tp"),
        P(None, "tp"),
        P("tp"),
        P(),
        P(),
        P("tp", None),
        P(),
        P(),
        P(None, EP),
        P(None, EP),
        P(EP, "tp"),
        P(EP, None),
        P(EP, None),
        P(EP, None, "tp"),
        P(EP, None, "tp"),
        P(EP, "tp", None),
    )
    return jax.shard_map(
        per_device, mesh=finer, in_specs=placed, out_specs=P(EP, "tp"), check_vma=False
    )
```

profile of v0, /device:TPU:8, one launch (start us, length us, event | category | flops | bytes accessed | tf_op | source)
XLA Modules:
  0.0 320.0 jit_solution(15933887718298431837)
XLA Ops:
  6.5 0.8 broadcast_add_fusion
  7.3 0.7 iota_compare_fusion.5
  8.7 0.7 convert_element_type.133
  9.4 0.7 convert_element_type.137
  10.0 0.8 fusion.43
  10.9 0.7 convert_element_type.131
  11.6 1.2 fusion.14
  12.7 1.3 multiply_reduce_fusion.2
  14.1 1.3 fusion.49
  15.5 0.1 copy.97
  15.5 0.1 fusion.60
  15.6 0.2 multiply_reduce_fusion.1
  15.8 0.1 copy.99
  15.8 0.9 fusion.47
  16.8 0.9 fusion.62
  17.7 0.8 subtract_add_fusion
  18.6 0.5 fusion.71
  19.1 0.3 fusion.13
  19.4 0.2 convolution_convert_fusion.1
  19.6 0.6 broadcast_in_dim.26
  20.2 9.0 %all-to-all-start = ((bf16[4,8,1024]{2,1,0:T(8,128)(2,1)}), bf16[4,8,1024]{2,1,0:T(8,128)(2,1)S(1)}, u32[]{:S(2)}, u32[]{:S(2)}) async-start(bf16[4,8,1024]{2,1,0:T(8,128)(2,1)} %broadcast_in_dim.26), calls=%async_computation | async-start | bytes 131072 | tf_op jit(solution)/shard_map/all_to_all | solution.py:14
  29.3 4.2 %all-to-all-done = bf16[4,8,1024]{2,1,0:T(8,128)(2,1)S(1)} async-done(((bf16[4,8,1024]{2,1,0:T(8,128)(2,1)}), bf16[4,8,1024]{2,1,0:T(8,128)(2,1)S(1)}, u32[]{:S(2)}, u32[]{:S(2)}) %all-to-all-start) | async-done | bytes 65568 | tf_op jit(solution)/shard_map/all_to_all | solution.py:14
  33.5 0.1 multiply_reduce_fusion
  33.6 0.7 multiply_convert_fusion
  34.4 85.2 %all-gather = s32[128,8,2]{1,2,0:T(2,128)S(1)} all-gather(s32[1,8,2]{1,2,0:T(2,128)S(1)} %bitcast.132), channel_id=1, replica_groups=mesh['ep_0'=16,'ep_1'=4,'ep_2'=2,'tp'=4] {'ep_0','ep_1','ep_2'}, dimensions={0}, use_global_device_ids=true | all-gather | bytes 8256 | tf_op jit(solution)/shard_map/all_gather | solution.py:154
  119.6 0.1 copy.104
  119.6 0.1 copy.107
  119.7 0.1 convert_reduce_fusion
  119.9 54.6 %all-gather.3.cloned.1.call-done = bf16[1024,1024]{1,0:T(8,128)(2,1)} async-done(((bf16[8,1024]{1,0:T(8,128)(2,1)}), bf16[1024,1024]{1,0:T(8,128)(2,1)}) %all-gather.3.cloned.1.call-update) | async-done | bytes 2097168 | tf_op jit(solution)/shard_map/all_gather | solution.py:153
  174.5 2.5 fusion.72
  177.0 2.0 fusion.7
  179.0 2.4 copy.100
  181.5 0.1 add.171
  181.6 0.1 add.172
  181.7 0.1 copy.108
  181.8 0.1 reduce_sum.139
  181.9 0.3 copy.105
  182.2 0.3 and.27
  182.5 1.0 copy.106
  183.5 1.3 mul.279
  184.8 3.6 %broadcast_in_dim.28 = bf16[1024,2,1024]{2,1,0:T(2,128)(2,1)} broadcast(bf16[1024,1024]{1,0:T(8,128)(2,1)S(1)} %copy-done.1), dimensions={0,2} | broadcast | bytes 6291456 | tf_op jit(solution)/shard_map/broadcast_in_dim | solution.py:169
  188.4 7.4 %reshape.353 = bf16[2048,1024]{1,0:T(8,128)(2,1)} reshape(bf16[1024,2,1024]{2,1,0:T(2,128)(2,1)} %broadcast_in_dim.28) | data formatting | bytes 8388608 | tf_op jit(solution)/shard_map/reshape | solution.py:169
  195.8 4.6 %fusion.2 = bf16[512,1024]{1,0:T(8,128)(2,1)S(1)} fusion(bf16[2048,1024]{1,0:T(8,128)(2,1)} %reshape.353, s32[2048]{0:T(1024)S(1)} %add_select_fusion), kind=kOutput, calls=%fused_computation.3 | convolution fusion | flops 2149056512 | bytes 5251072 | tf_op jit(solution)/shard_map/dot_general | solution.py:170
  200.4 0.4 reshape.354
  200.9 2.3 convolution_bitcast_fusion.1
  203.2 2.3 convolution_convert_fusion
  205.5 1.1 copy.138
  206.6 5.0 %all-to-all-start.1 = ((bf16[4,128,1,4,256]{4,1,3,2,0:T(8,128)(2,1)}), bf16[4,128,1,4,256]{4,1,3,2,0:T(8,128)(2,1)S(1)}, u32[]{:S(2)}, u32[]{:S(2)}) async-start(bf16[4,128,1,4,256]{4,1,3,2,0:T(8,128)(2,1)} %bitcast.122), calls=%async_computation.4 | async-start | bytes 2097152 | tf_op jit(solution)/shard_map/all_to_all | solution.py:30
  211.6 0.7 reduce-scatter.6.cloned.1.call-update
  212.3 13.3 %all-to-all-done.1 = bf16[4,128,1,4,256]{4,1,3,2,0:T(8,128)(2,1)S(1)} async-done(((bf16[4,128,1,4,256]{4,1,3,2,0:T(8,128)(2,1)}), bf16[4,128,1,4,256]{4,1,3,2,0:T(8,128)(2,1)S(1)}, u32[]{:S(2)}, u32[]{:S(2)}) %all-to-all-start.1) | async-done | bytes 1048608 | tf_op jit(solution)/shard_map/all_to_all | solution.py:30
  225.6 0.2 reduce_sum.140
  225.9 0.9 copy.113
  226.8 11.5 %all-to-all-start.2 = ((bf16[128,1,4,256]{3,2,1,0:T(4,128)(2,1)}), bf16[128,1,4,256]{3,2,1,0:T(4,128)(2,1)S(1)}, u32[]{:S(2)}, u32[]{:S(2)}) async-start(bf16[128,1,4,256]{3,2,1,0:T(4,128)(2,1)} %copy.113), calls=%async_computation.5 | async-start | bytes 524288 | tf_op jit(solution)/shard_map/all_to_all | solution.py:183
  238.3 0.1 copy.101
  238.3 0.1 eq.76
  238.4 0.2 convert_reduce_fusion.2
  238.6 0.1 reduce_sum.135
  238.7 0.1 copy.103
  238.8 0.1 select_reduce_fusion
  238.9 44.9 %reduce-scatter.6.cloned.1.call-done = f32[4,8,256]{2,1,0:T(8,128)} async-done(((f32[64,8,256]{2,1,0:T(8,128)}), f32[4,8,256]{2,1,0:T(8,128)}) %reduce-scatter.6.cloned.1.call-update) | async-done | bytes 32784 | tf_op jit(solution)/shard_map/reduce_scatter | solution.py:40
  283.8 0.1 fusion.18
  284.0 0.1 reshape.360
  284.1 27.9 %reduce-scatter.8.cloned.1.call-done = f32[1,8,256]{2,1,0:T(8,128)} async-done(((f32[4,8,256]{2,1,0:T(8,128)}), f32[1,8,256]{2,1,0:T(8,128)}) %reduce-scatter.8.cloned.1.call-update) | async-done | bytes 8208 | tf_op jit(solution)/shard_map/reduce_scatter | solution.py:40
  312.0 1.5 fusion.12
  (52 shorter events, 0.3 us)
Async XLA Ops:
  6.5 12.0 %copy-start = (bf16[8,512,1,128]{3,1,2,0:T(8,128)(2,1)S(1)}, bf16[8,512,1,128]{3,1,2,0:T(8,128)(2,1)}, u32[]{:S(2)}) copy-start(bf16[8,512,1,128]{3,1,2,0:T(8,128)(2,1)} %param.26) | copy-start | bytes 3145732
  6.5 12.5 %copy-start.12 = (bf16[8,512,1,128]{3,1,2,0:T(8,128)(2,1)S(1)}, bf16[8,512,1,128]{3,1,2,0:T(8,128)(2,1)}, u32[]{:S(2)}) copy-start(bf16[8,512,1,128]{3,1,2,0:T(8,128)(2,1)} %param.27) | copy-start | bytes 3145732
  6.5 12.8 %copy-start.2 = (bf16[256,1024]{1,0:T(8,128)(2,1)S(1)}, bf16[256,1024]{1,0:T(8,128)(2,1)}, u32[]{:S(2)}) copy-start(bf16[256,1024]{1,0:T(8,128)(2,1)} %param.37) | copy-start | bytes 1572868
  12.7 16.5 %copy-start.10 = (bf16[1024]{0:T(1024)(128)(2,1)S(1)}, bf16[1024]{0:T(1024)(128)(2,1)}, u32[]{:S(2)}) copy-start(bf16[1024]{0:T(1024)(128)(2,1)} %param.38) | copy-start | bytes 6148
  12.7 20.7 %copy-start.3 = (bf16[8,1024]{1,0:T(8,128)(2,1)S(1)}, bf16[8,1024]{1,0:T(8,128)(2,1)}, u32[]{:S(2)}) copy-start(bf16[8,1024]{1,0:T(8,128)(2,1)} %param.24) | copy-start | bytes 49156
  14.1 20.3 %copy-start.8 = (s32[8,2]{0,1:T(2,128)S(1)}, s32[8,2]{0,1:T(2,128)}, u32[]{:S(2)}) copy-start(s32[8,2]{0,1:T(2,128)} %param.43) | copy-start | bytes 196
  15.4 159.1 %copy-start.4 = (bf16[1024,32]{0,1:T(8,128)(2,1)S(1)}, bf16[1024,32]{0,1:T(8,128)(2,1)}, u32[]{:S(2)}) copy-start(bf16[1024,32]{0,1:T(8,128)(2,1)} %param.40) | copy-start | bytes 196612
  19.4 157.6 %copy-start.5 = (bf16[1024,32]{0,1:T(8,128)(2,1)S(1)}, bf16[1024,32]{0,1:T(8,128)(2,1)}, u32[]{:S(2)}) copy-start(bf16[1024,32]{0,1:T(8,128)(2,1)} %param.41) | copy-start | bytes 196612
  19.4 157.6 %copy-start.7 = (bf16[32,256]{1,0:T(8,128)(2,1)S(1)}, bf16[32,256]{1,0:T(8,128)(2,1)}, u32[]{:S(2)}) copy-start(bf16[32,256]{1,0:T(8,128)(2,1)} %param.42) | copy-start | bytes 49156
  20.2 13.2 %all-to-all-start = ((bf16[4,8,1024]{2,1,0:T(8,128)(2,1)}), bf16[4,8,1024]{2,1,0:T(8,128)(2,1)S(1)}, u32[]{:S(2)}, u32[]{:S(2)}) async-start(bf16[4,8,1024]{2,1,0:T(8,128)(2,1)} %broadcast_in_dim.26), calls=%async_computation | async-start | bytes 131072 | tf_op jit(solution)/shard_map/all_to_all | solution.py:14
  29.3 145.2 %all-gather.3.cloned.1.call-start = ((), (), s32[]{:S(2)}) async-start(), calls=%async_computation.6 | async-start | bytes 2113536 | tf_op jit(solution)/shard_map/all_gather | solution.py:153
  34.3 177.3 %reduce-scatter.4.cloned.1.call-start = ((), (), s32[]{:S(2)}) async-start(), calls=%async_computation.7 | async-start | bytes 1572864 | tf_op jit(solution)/shard_map/reduce_scatter | solution.py:40
  174.5 2.5 copy-start.1
  206.6 32.2 %copy-start.11 = (bf16[1024]{0:T(1024)(128)(2,1)S(1)}, bf16[1024]{0:T(1024)(128)(2,1)}, u32[]{:S(2)}) copy-start(bf16[1024]{0:T(1024)(128)(2,1)} %param.39) | copy-start | bytes 6148
  206.6 32.2 %copy-start.9 = (f32[8,2]{0,1:T(2,128)S(1)}, f32[8,2]{0,1:T(2,128)}, u32[]{:S(2)}) copy-start(f32[8,2]{0,1:T(2,128)} %param.44) | copy-start | bytes 196
  206.6 77.2 %copy-start.6 = (bf16[8,1024]{1,0:T(8,128)(2,1)S(1)}, bf16[8,1024]{1,0:T(8,128)(2,1)}, u32[]{:S(2)}) copy-start(bf16[8,1024]{1,0:T(8,128)(2,1)} %multiply_convert_fusion) | copy-start | bytes 49156
  206.6 19.0 %all-to-all-start.1 = ((bf16[4,128,1,4,256]{4,1,3,2,0:T(8,128)(2,1)}), bf16[4,128,1,4,256]{4,1,3,2,0:T(8,128)(2,1)S(1)}, u32[]{:S(2)}, u32[]{:S(2)}) async-start(bf16[4,128,1,4,256]{4,1,3,2,0:T(8,128)(2,1)} %bitcast.122), calls=%async_computation.4 | async-start | bytes 2097152 | tf_op jit(solution)/shard_map/all_to_all | solution.py:30
  211.6 72.2 %reduce-scatter.6.cloned.1.call-start = ((), (), s32[]{:S(2)}) async-start(), calls=%async_computation.8 | async-start | bytes 557056 | tf_op jit(solution)/shard_map/reduce_scatter | solution.py:40
  226.8 57.2 %all-to-all-start.2 = ((bf16[128,1,4,256]{3,2,1,0:T(4,128)(2,1)}), bf16[128,1,4,256]{3,2,1,0:T(4,128)(2,1)S(1)}, u32[]{:S(2)}, u32[]{:S(2)}) async-start(bf16[128,1,4,256]{3,2,1,0:T(4,128)(2,1)} %copy.113), calls=%async_computation.5 | async-start | bytes 524288 | tf_op jit(solution)/shard_map/all_to_all | solution.py:183
  238.2 73.8 %reduce-scatter.8.cloned.1.call-start = ((), (), s32[]{:S(2)}) async-start(), calls=%async_computation.9 | async-start | bytes 40960 | tf_op jit(solution)/shard_map/reduce_scatter | solution.py:40
Sparse Core Ops, SparseCore 0:
  34.4 140.0 all-gather.2
  181.6 15.1 reduce-scatter.3
  215.2 68.5 reduce-scatter.5
  286.4 25.4 reduce-scatter.7
where the time goes:
time: 321 us; the launch traced here: 320 us
  waiting for transfers between devices  146 us (45%)
  blocking collectives  85.2 us (27%)
  starting transfers between devices  25.5 us (8%)
  matrix products  21.1 us (7%)
  local copies, waits for them, and re-layouts  20.6 us (6%)
  between operations  14 us (4%)
  other arithmetic  7.9 us (2%)
    all_gather x1, blocking collectives, per_device(): lax.all_gather(routes, EP, axis=0, tiled=True)  85.2 us
    reduce_scatter x3, waiting for transfers between devices, sum_in_order(): tiles = lax.psum_scatter(tiles, axes[k], scatter_dimension=0, tiled=True)  72.8 us
    all_gather x1, waiting for transfers between devices, per_device(): lax.all_gather(ffn_in, EP, axis=0, tiled=True)  54.6 us
    all_to_all x1, waiting for transfers between devices, summed_on_arrival(): tiles = lax.all_to_all(cut_along(shard, dim, peers), axis, 0, 0, tiled=True)  13.3 us
    all_to_all x1, starting transfers between devices, per_device(): lax.all_to_all(results, EP, split_axis=0, concat_axis=0, tiled=True)  11.5 us
    all_to_all x1, starting transfers between devices, copy_for_each(): lax.all_to_all(jnp.broadcast_to(shard[None], (peers, *shard.shape)), axis...  9.04 us
    reshape x1, local copies, waits for them, and re-layouts, per_device(): repeated_all = jnp.repeat(gathered_rows, topk, axis=0)  7.4 us
  transfers between devices with their start and end apart: 7, of which 5 were waited for; matrix products, arithmetic and copies ran while one was open for 9% of the time, Pallas kernels for 0%

commit v1 on v0

--- a/solution.py
+++ b/solution.py
@@ -150,7 +150,15 @@
     slot_rank = jnp.sum(jnp.logical_and(same_expert, earlier), axis=1)
     slot_index = flat_route * CAP + slot_rank
     gathered_rows, gathered_routes = (
-        lax.all_gather(ffn_in, EP, axis=0, tiled=True),
+        jnp.concatenate(
+            lax.all_to_all(
+                jnp.stack([ffn_in for _ in range(lax.axis_size(EP))], axis=0),
+                axis_name=EP,
+                split_axis=0,
+                concat_axis=0,
+            ),
+            0,
+        ),
         lax.all_gather(routes, EP, axis=0, tiled=True),
     )
     pre_gate = jnp.dot(gathered_rows, shared_gate, preferred_element_type=jnp.float32)

time: 321 us -> 367 us (1.14)
  blocking collectives: 85.2 us -> 167 us
  waiting for transfers between devices: 146 us -> 91.5 us
  starting transfers between devices: 25.5 us -> 44.5 us
    all_gather x1, blocking collectives: 85.2 us -> 167 us  [per_device(): lax.all_gather(routes, EP, axis=0, tiled=True)]
    all_gather x1 -> x0, waiting for transfers between devices: 54.6 us -> none  [per_device(): lax.all_gather(ffn_in, EP, axis=0, tiled=True)]
    all_to_all x0 -> x1, starting transfers between devices: none -> 15.8 us  [per_device(): lax.all_to_all(jnp.stack([ffn_in for _ in range(lax.axis_size(EP))], axis...]
  transfers between devices with their start and end apart: 7 -> 7, of which waited for: 5 -> 4; matrix products, arithmetic and copies ran while one was open for 9% -> 7% of each run, Pallas kernels for 0% -> 0%
where the time goes in v1:
time: 367 us; the launch traced here: 365 us
  blocking collectives  167 us (46%)
  waiting for transfers between devices  91.5 us (25%)
  starting transfers between devices  44.5 us (12%)
  local copies, waits for them, and re-layouts  22 us (6%)
  matrix products  19.4 us (5%)
  between operations  14 us (4%)
  other arithmetic  7.3 us (2%)
    all_gather x1, blocking collectives, per_device(): lax.all_gather(routes, EP, axis=0, tiled=True)  167 us
    reduce_scatter x3, waiting for transfers between devices, sum_in_order(): tiles = lax.psum_scatter(tiles, axes[k], scatter_dimension=0, tiled=True)  72.9 us
    all_to_all x1, starting transfers between devices, per_device(): lax.all_to_all(jnp.stack([ffn_in for _ in range(lax.axis_size(EP))], axis...  15.8 us
    all_to_all x1, starting transfers between devices, per_device(): lax.all_to_all(results, EP, split_axis=0, concat_axis=0, tiled=True)  14.4 us
    all_to_all x1, waiting for transfers between devices, summed_on_arrival(): tiles = lax.all_to_all(cut_along(shard, dim, peers), axis, 0, 0, tiled=True)  13.6 us
    all_to_all x1, starting transfers between devices, copy_for_each(): lax.all_to_all(jnp.broadcast_to(shard[None], (peers, *shard.shape)), axis...  9.04 us
  transfers between devices with their start and end apart: 7, of which 4 were waited for; matrix products, arithmetic and copies ran while one was open for 7% of the time, Pallas kernels for 0%

profile of v1, /device:TPU:8, one launch (start us, length us, event | category | flops | bytes accessed | tf_op | source)
XLA Modules:
  0.0 365.3 jit_solution(11416481461757201476)
XLA Ops:
  6.5 0.8 broadcast_add_fusion
  7.3 0.7 iota_compare_fusion.5
  8.7 0.7 convert_element_type.133
  9.4 0.7 convert_element_type.137
  10.0 0.8 fusion.43
  10.9 0.7 convert_element_type.131
  11.6 1.2 fusion.14
  12.7 1.3 multiply_reduce_fusion.2
  14.1 1.4 fusion.49
  15.4 0.1 copy.97
  15.5 0.1 fusion.60
  15.6 0.2 multiply_reduce_fusion.1
  15.8 0.1 copy.99
  15.8 0.9 fusion.47
  16.8 0.9 fusion.62
  17.7 0.8 subtract_add_fusion
  18.5 0.5 fusion.75
  19.1 0.3 fusion.13
  19.4 0.2 convolution_convert_fusion.1
  19.6 0.6 broadcast_in_dim.26
  20.2 9.0 %all-to-all-start = ((bf16[4,8,1024]{2,1,0:T(8,128)(2,1)}), bf16[4,8,1024]{2,1,0:T(8,128)(2,1)S(1)}, u32[]{:S(2)}, u32[]{:S(2)}) async-start(bf16[4,8,1024]{2,1,0:T(8,128)(2,1)} %broadcast_in_dim.26), calls=%async_computation | async-start | bytes 131072 | tf_op jit(solution)/shard_map/all_to_all | solution.py:14
  29.3 4.2 %all-to-all-done = bf16[4,8,1024]{2,1,0:T(8,128)(2,1)S(1)} async-done(((bf16[4,8,1024]{2,1,0:T(8,128)(2,1)}), bf16[4,8,1024]{2,1,0:T(8,128)(2,1)S(1)}, u32[]{:S(2)}, u32[]{:S(2)}) %all-to-all-start) | async-done | bytes 65568 | tf_op jit(solution)/shard_map/all_to_all | solution.py:14
  33.5 0.1 multiply_reduce_fusion
  33.6 0.1 multiply_convert_fusion
  33.7 1.6 stack.2
  35.3 15.8 %all-to-all-start.1 = ((bf16[128,8,1024]{2,1,0:T(8,128)(2,1)}), bf16[128,8,1024]{2,1,0:T(8,128)(2,1)S(1)}, u32[]{:S(2)}, u32[]{:S(2)}) async-start(bf16[128,8,1024]{2,1,0:T(8,128)(2,1)} %stack.2), calls=%async_computation.1 | async-start | bytes 4194304 | tf_op jit(solution)/shard_map/all_to_all | solution.py:154
  51.2 166.7 %all-gather = s32[128,8,2]{1,2,0:T(2,128)S(1)} all-gather(s32[1,8,2]{1,2,0:T(2,128)S(1)} %bitcast.137), channel_id=1, replica_groups=mesh['ep_0'=16,'ep_1'=4,'ep_2'=2,'tp'=4] {'ep_0','ep_1','ep_2'}, dimensions={0}, use_global_device_ids=true | all-gather | bytes 8256 | tf_op jit(solution)/shard_map/all_gather | solution.py:162
  217.9 0.1 copy.107
  218.0 0.1 convert_reduce_fusion
  218.2 0.7 fusion.65
  218.9 2.0 fusion.7
  220.9 2.4 copy.100
  223.4 0.1 add.171
  223.5 0.1 add.172
  223.6 0.1 copy.108
  223.7 0.1 reduce_sum.139
  223.8 0.3 copy.105
  224.1 0.3 and.27
  224.4 1.0 copy.106
  225.5 1.3 mul.279
  226.8 3.6 broadcast_in_dim.28
  230.3 7.2 %reshape.359 = bf16[2048,1024]{1,0:T(8,128)(2,1)} reshape(bf16[1024,2,1024]{2,1,0:T(2,128)(2,1)} %broadcast_in_dim.28) | data formatting | bytes 8388608 | tf_op jit(solution)/shard_map/reshape | solution.py:177
  237.6 4.6 %fusion.2 = bf16[512,1024]{1,0:T(8,128)(2,1)S(1)} fusion(bf16[2048,1024]{1,0:T(8,128)(2,1)} %reshape.359, s32[2048]{0:T(1024)S(1)} %add_select_fusion), kind=kOutput, calls=%fused_computation.3 | convolution fusion | flops 2149056512 | bytes 5251072 | tf_op jit(solution)/shard_map/dot_general | solution.py:178
  242.2 0.4 reshape.360
  242.6 2.3 convolution_bitcast_fusion.1
  244.9 2.3 convolution_convert_fusion
  247.3 1.1 copy.138
  248.4 5.1 %all-to-all-start.2 = ((bf16[4,128,1,4,256]{4,1,3,2,0:T(8,128)(2,1)}), bf16[4,128,1,4,256]{4,1,3,2,0:T(8,128)(2,1)S(1)}, u32[]{:S(2)}, u32[]{:S(2)}) async-start(bf16[4,128,1,4,256]{4,1,3,2,0:T(8,128)(2,1)} %bitcast.126), calls=%async_computation.5 | async-start | bytes 2097152 | tf_op jit(solution)/shard_map/all_to_all | solution.py:30
  253.5 0.7 reduce-scatter.6.cloned.1.call-update
  254.2 13.6 %all-to-all-done.2 = bf16[4,128,1,4,256]{4,1,3,2,0:T(8,128)(2,1)S(1)} async-done(((bf16[4,128,1,4,256]{4,1,3,2,0:T(8,128)(2,1)}), bf16[4,128,1,4,256]{4,1,3,2,0:T(8,128)(2,1)S(1)}, u32[]{:S(2)}, u32[]{:S(2)}) %all-to-all-start.2) | async-done | bytes 1048608 | tf_op jit(solution)/shard_map/all_to_all | solution.py:30
  267.9 0.2 reduce_sum.140
  268.1 0.9 copy.113
  269.0 14.4 %all-to-all-start.3 = ((bf16[128,1,4,256]{3,2,1,0:T(4,128)(2,1)}), bf16[128,1,4,256]{3,2,1,0:T(4,128)(2,1)S(1)}, u32[]{:S(2)}, u32[]{:S(2)}) async-start(bf16[128,1,4,256]{3,2,1,0:T(4,128)(2,1)} %copy.113), calls=%async_computation.6 | async-start | bytes 524288 | tf_op jit(solution)/shard_map/all_to_all | solution.py:191
  283.5 0.1 copy.101
  283.6 0.1 eq.76
  283.6 0.2 convert_reduce_fusion.2
  283.8 0.1 reduce_sum.135
  283.9 0.1 copy.103
  284.1 0.1 select_reduce_fusion
  284.1 44.3 %reduce-scatter.6.cloned.1.call-done = f32[4,8,256]{2,1,0:T(8,128)} async-done(((f32[64,8,256]{2,1,0:T(8,128)}), f32[4,8,256]{2,1,0:T(8,128)}) %reduce-scatter.6.cloned.1.call-update) | async-done | bytes 32784 | tf_op jit(solution)/shard_map/reduce_scatter | solution.py:40
  328.5 0.1 fusion.18
  328.6 0.1 reshape.366
  328.7 28.6 %reduce-scatter.8.cloned.1.call-done = f32[1,8,256]{2,1,0:T(8,128)} async-done(((f32[4,8,256]{2,1,0:T(8,128)}), f32[1,8,256]{2,1,0:T(8,128)}) %reduce-scatter.8.cloned.1.call-update) | async-done | bytes 8208 | tf_op jit(solution)/shard_map/reduce_scatter | solution.py:40
  357.3 1.5 fusion.12
  (48 shorter events, 0.4 us)
Async XLA Ops:
  6.5 12.0 %copy-start = (bf16[8,512,1,128]{3,1,2,0:T(8,128)(2,1)S(1)}, bf16[8,512,1,128]{3,1,2,0:T(8,128)(2,1)}, u32[]{:S(2)}) copy-start(bf16[8,512,1,128]{3,1,2,0:T(8,128)(2,1)} %param.26) | copy-start | bytes 3145732
  6.5 12.5 %copy-start.10 = (bf16[8,512,1,128]{3,1,2,0:T(8,128)(2,1)S(1)}, bf16[8,512,1,128]{3,1,2,0:T(8,128)(2,1)}, u32[]{:S(2)}) copy-start(bf16[8,512,1,128]{3,1,2,0:T(8,128)(2,1)} %param.27) | copy-start | bytes 3145732
  6.5 12.8 %copy-start.1 = (bf16[256,1024]{1,0:T(8,128)(2,1)S(1)}, bf16[256,1024]{1,0:T(8,128)(2,1)}, u32[]{:S(2)}) copy-start(bf16[256,1024]{1,0:T(8,128)(2,1)} %param.37) | copy-start | bytes 1572868
  12.7 16.5 %copy-start.8 = (bf16[1024]{0:T(1024)(128)(2,1)S(1)}, bf16[1024]{0:T(1024)(128)(2,1)}, u32[]{:S(2)}) copy-start(bf16[1024]{0:T(1024)(128)(2,1)} %param.38) | copy-start | bytes 6148
  12.7 20.7 %copy-start.2 = (bf16[8,1024]{1,0:T(8,128)(2,1)S(1)}, bf16[8,1024]{1,0:T(8,128)(2,1)}, u32[]{:S(2)}) copy-start(bf16[8,1024]{1,0:T(8,128)(2,1)} %param.24) | copy-start | bytes 49156
  20.2 13.2 %all-to-all-start = ((bf16[4,8,1024]{2,1,0:T(8,128)(2,1)}), bf16[4,8,1024]{2,1,0:T(8,128)(2,1)S(1)}, u32[]{:S(2)}, u32[]{:S(2)}) async-start(bf16[4,8,1024]{2,1,0:T(8,128)(2,1)} %broadcast_in_dim.26), calls=%async_computation | async-start | bytes 131072 | tf_op jit(solution)/shard_map/all_to_all | solution.py:14
  35.3 15.9 %copy-start.6 = (s32[8,2]{0,1:T(2,128)S(1)}, s32[8,2]{0,1:T(2,128)}, u32[]{:S(2)}) copy-start(s32[8,2]{0,1:T(2,128)} %param.43) | copy-start | bytes 196
  35.3 182.9 %copy-start.3 = (bf16[1024,32]{0,1:T(8,128)(2,1)S(1)}, bf16[1024,32]{0,1:T(8,128)(2,1)}, u32[]{:S(2)}) copy-start(bf16[1024,32]{0,1:T(8,128)(2,1)} %param.40) | copy-start | bytes 196612
  35.3 182.8 %all-to-all-start.1 = ((bf16[128,8,1024]{2,1,0:T(8,128)(2,1)}), bf16[128,8,1024]{2,1,0:T(8,128)(2,1)S(1)}, u32[]{:S(2)}, u32[]{:S(2)}) async-start(bf16[128,8,1024]{2,1,0:T(8,128)(2,1)} %stack.2), calls=%async_computation.1 | async-start | bytes 4194304 | tf_op jit(solution)/shard_map/all_to_all | solution.py:154
  51.1 167.8 %copy-start.4 = (bf16[1024,32]{0,1:T(8,128)(2,1)S(1)}, bf16[1024,32]{0,1:T(8,128)(2,1)}, u32[]{:S(2)}) copy-start(bf16[1024,32]{0,1:T(8,128)(2,1)} %param.41) | copy-start | bytes 196612
  51.1 167.8 %copy-start.5 = (bf16[32,256]{1,0:T(8,128)(2,1)S(1)}, bf16[32,256]{1,0:T(8,128)(2,1)}, u32[]{:S(2)}) copy-start(bf16[32,256]{1,0:T(8,128)(2,1)} %param.42) | copy-start | bytes 49156
  51.1 202.4 %reduce-scatter.4.cloned.1.call-start = ((), (), s32[]{:S(2)}) async-start(), calls=%async_computation.7 | async-start | bytes 1572864 | tf_op jit(solution)/shard_map/reduce_scatter | solution.py:40
  248.4 35.6 %copy-start.9 = (bf16[1024]{0:T(1024)(128)(2,1)S(1)}, bf16[1024]{0:T(1024)(128)(2,1)}, u32[]{:S(2)}) copy-start(bf16[1024]{0:T(1024)(128)(2,1)} %param.39) | copy-start | bytes 6148
  248.4 35.7 %copy-start.7 = (f32[8,2]{0,1:T(2,128)S(1)}, f32[8,2]{0,1:T(2,128)}, u32[]{:S(2)}) copy-start(f32[8,2]{0,1:T(2,128)} %param.44) | copy-start | bytes 196
  248.4 19.5 %all-to-all-start.2 = ((bf16[4,128,1,4,256]{4,1,3,2,0:T(8,128)(2,1)}), bf16[4,128,1,4,256]{4,1,3,2,0:T(8,128)(2,1)S(1)}, u32[]{:S(2)}, u32[]{:S(2)}) async-start(bf16[4,128,1,4,256]{4,1,3,2,0:T(8,128)(2,1)} %bitcast.126), calls=%async_computation.5 | async-start | bytes 2097152 | tf_op jit(solution)/shard_map/all_to_all | solution.py:30
  253.5 75.0 %reduce-scatter.6.cloned.1.call-start = ((), (), s32[]{:S(2)}) async-start(), calls=%async_computation.8 | async-start | bytes 557056 | tf_op jit(solution)/shard_map/reduce_scatter | solution.py:40
  269.0 59.6 %all-to-all-start.3 = ((bf16[128,1,4,256]{3,2,1,0:T(4,128)(2,1)}), bf16[128,1,4,256]{3,2,1,0:T(4,128)(2,1)S(1)}, u32[]{:S(2)}, u32[]{:S(2)}) async-start(bf16[128,1,4,256]{3,2,1,0:T(4,128)(2,1)} %copy.113), calls=%async_computation.6 | async-start | bytes 524288 | tf_op jit(solution)/shard_map/all_to_all | solution.py:191
  283.4 73.9 %reduce-scatter.8.cloned.1.call-start = ((), (), s32[]{:S(2)}) async-start(), calls=%async_computation.9 | async-start | bytes 40960 | tf_op jit(solution)/shard_map/reduce_scatter | solution.py:40
Sparse Core Ops, SparseCore 0:
  223.5 16.6 reduce-scatter.3
  257.1 71.3 reduce-scatter.5
  331.3 25.9 reduce-scatter.7
